TPU v7x, 32 devices: a whole 2x2x4 slice. The times are simulated.
32 devices in a mesh: rep: 2 (over x), fs: 8 (over z, y), tp: 2 (over core).
Axes of the slice: x: 2, y: 2, z: 4, core: 2. Of those that a mesh axis runs over, the one named last changes fastest.
Arguments:
- residual: bfloat16 [8192, 2048], P(('rep', 'fs', 'tp')), may hold values from -6 to 6
- mixer_gain: float32 [2048], replicated, may hold values from 0.1 to 1.9
- gating_proj: bfloat16 [2048, 2048], P('fs', 'tp'), may hold values from -0.125 to 0.125
- spatial_proj: bfloat16 [2048, 2048], P('fs', 'tp'), as said below
- spatial_gain: float32 [2048], replicated, may hold values from 0.1 to 1.9
- spatial_bias: float32 [2048], replicated, may hold values from -3 to 3
- spatial_mix: bfloat16 [32, 128, 128], replicated, may hold values from -0.5 to 0.5
- spatial_offset: float32 [32, 128], replicated, may hold values from 0.5 to 1.5
- mixer_out: bfloat16 [2048, 2048], P('tp', 'fs'), may hold values from -0.125 to 0.125
- channel_gain: float32 [2048], replicated, may hold values from 0.1 to 1.9
- gate_proj: bfloat16 [2048, 2816], P('fs', 'tp'), may hold values from -0.125 to 0.125
- up_proj: bfloat16 [2048, 2816], P('fs', 'tp'), may hold values from -0.125 to 0.125
- conv_taps: float32 [3, 2816], replicated, may hold values from -3.5 to 3.5
- down_proj: bfloat16 [2816, 2048], P('tp', 'fs'), may hold values from -0.109375 to 0.109375
Outputs:
- layer_out: bfloat16 [8192, 2048], P(('rep', 'fs', 'tp'))
Inputs may be any that keep to these rules, and one draw needn't show every extreme that they name: `spatial_proj`: entries are bounded in magnitude by 56 / sqrt(2048).
All inputs are finite; a program needn't handle non-finite values.
Results may differ from a plain program's by a relative error of at most 0.015.
Values may be sent and summed in bfloat16 or wider, within the bound.
A program may use at most 128 MiB of HBM per device.

v0:
```python
import jax
import jax.numpy as jnp
from jax import lax
from jax.sharding import PartitionSpec as P

HEAD = 64
GROUP = 2048
BLOCK = 128
SEGMENT = 64
KCONV = 3
SEQ_LEN = 256


def round_trip(value):
    return lax.optimization_barrier(value.astype(jnp.bfloat16)).astype(jnp.float32)


def rms_normed(value, gain):
    wide = value.astype(jnp.float32)
    scale = lax.rsqrt(jnp.mean(wide * wide, axis=-1, keepdims=True) + 1e-06)
    return (wide * scale * gain).astype(jnp.bfloat16)


def fold_pair(normed, pieces):
    first = jnp.dot(normed, pieces[0], preferred_element_type=jnp.float32)
    second = jnp.dot(normed, pieces[1], preferred_element_type=jnp.float32)
    return (first, second)


def on_device(
    residual,
    mixer_gain,
    gating_proj,
    spatial_proj,
    spatial_gain,
    spatial_bias,
    spatial_mix,
    spatial_offset,
    mixer_out,
    channel_gain,
    gate_proj,
    up_proj,
    conv_taps,
    down_proj,
):
    position = lax.axis_index("tp")
    rows = lax.all_gather(residual, "tp", axis=0, tiled=True)
    group_rows = rows.shape[0]
    normed = rms_normed(rows, mixer_gain)
    width = gating_proj.shape[1]
    gating, spatial = fold_pair(
        normed,
        (
            lax.all_gather(gating_proj, "fs", axis=0, tiled=True),
            lax.all_gather(spatial_proj, "fs", axis=0, tiled=True),
        ),
    )
    act_u = jax.nn.gelu(round_trip(gating))
    act_v = jax.nn.gelu(round_trip(spatial))
    total, squares = lax.psum((jnp.sum(act_v, axis=-1), jnp.sum(act_v * act_v, axis=-1)), "tp")
    mean = (total / GROUP)[:, None]
    var = (squares / GROUP)[:, None] - mean * mean
    gain_here = lax.dynamic_slice_in_dim(spatial_gain, position * width, width)
    bias_here = lax.dynamic_slice_in_dim(spatial_bias, position * width, width)
    vnorm = ((act_v - mean) * lax.rsqrt(var + 1e-05) * gain_here + bias_here).astype(jnp.bfloat16)
    heads_here = width // HEAD
    mix_here = lax.dynamic_slice_in_dim(spatial_mix, position * heads_here, heads_here, 0)
    offset_here = lax.dynamic_slice_in_dim(spatial_offset, position * heads_here, heads_here, 0)
    place = jnp.arange(BLOCK) // SEGMENT
    allowed = place[None, :] <= place[:, None]
    weights = jnp.where(allowed[None], mix_here, jnp.zeros_like(mix_here))
    blocks = vnorm.reshape(group_rows // BLOCK, BLOCK, heads_here, HEAD)
    mixed = jnp.einsum("hij,njhd->nihd", weights, blocks, preferred_element_type=jnp.float32)
    mixed = mixed + offset_here.T[None, :, :, None]
    gated = (act_u * mixed.reshape(group_rows, width)).astype(jnp.bfloat16)
    out_whole = lax.all_gather(mixer_out, "fs", axis=1, tiled=True)
    part = gated
    mixer_part = lax.psum_scatter(
        jnp.dot(part, out_whole, preferred_element_type=jnp.float32).astype(jnp.bfloat16),
        "tp",
        scatter_dimension=0,
        tiled=True,
    ).astype(jnp.float32)
    middle = (residual.astype(jnp.float32) + mixer_part).astype(jnp.bfloat16)
    rows2 = lax.all_gather(middle, "tp", axis=0, tiled=True)
    normed2 = rms_normed(rows2, channel_gain)
    units = gate_proj.shape[1]
    gate, up = fold_pair(
        normed2,
        (
            lax.all_gather(gate_proj, "fs", axis=0, tiled=True),
            lax.all_gather(up_proj, "fs", axis=0, tiled=True),
        ),
    )
    gate = round_trip(gate)
    up = round_trip(up)
    taps_here = lax.dynamic_slice_in_dim(conv_taps, position * units, units, 1)
    offset = jnp.arange(group_rows) % SEQ_LEN
    conv = taps_here[KCONV - 1] * gate
    for lag in range(1, KCONV):
        shifted = jnp.concatenate([jnp.zeros((lag, units), jnp.float32), gate[:-lag]], axis=0)
        shifted = jnp.where((offset >= lag)[:, None], shifted, 0.0)
        conv = conv + taps_here[KCONV - 1 - lag] * shifted
    hidden = (jax.nn.silu(conv) * up).astype(jnp.bfloat16)
    down_whole = lax.all_gather(down_proj, "fs", axis=1, tiled=True)
    part = hidden
    channel_part = lax.psum_scatter(
        jnp.dot(part, down_whole, preferred_element_type=jnp.float32).astype(jnp.bfloat16),
        "tp",
        scatter_dimension=0,
        tiled=True,
    ).astype(jnp.float32)
    return (middle.astype(jnp.float32) + channel_part).astype(jnp.bfloat16)


def solution(mesh):
    in_specs = (
        P(("rep", "fs", "tp"), None),
        P(),
        P("fs", "tp"),
        P("fs", "tp"),
        P(),
        P(),
        P(),
        P(),
        P("tp", "fs"),
        P(),
        P("fs", "tp"),
        P("fs", "tp"),
        P(),
        P("tp", "fs"),
    )
    out_specs = P(("rep", "fs", "tp"), None)
    return jax.shard_map(
        on_device, mesh=mesh, in_specs=in_specs, out_specs=out_specs, check_vma=False
    )
```

profile of v0, /device:TPU:0, one launch (start us, length us, event | category | flops | bytes accessed | tf_op | source)
XLA Modules:
  0.0 586.4 jit_solution(640272475224607658)
XLA Ops:
  6.5 0.7 all-gather.9.cloned.1.call-update
  7.3 0.0 all-gather.13.cloned.1.call-start
  7.3 0.7 all-gather.13.cloned.1.call-update
  8.0 0.0 all-gather.11.cloned.1.call-start
  8.1 0.7 all-gather.11.cloned.1.call-update
  8.8 0.0 all-gather.15.cloned.1.call-start
  8.8 0.5 all-gather.15.cloned.1.call-update
  9.3 0.0 reduce-scatter.3.cloned.1.call-start
  9.4 0.1 broadcast_compare_fusion
  9.5 12.7 %all-gather.9.cloned.1.call-done = bf16[512,2048]{1,0:T(8,128)(2,1)} async-done(((bf16[256,2048]{1,0:T(8,128)(2,1)}), bf16[512,2048]{1,0:T(8,128)(2,1)}) %all-gather.9.cloned.1.call-update) | async-done | bytes 2097168 | tf_op jit(solution)/shard_map/all_gather | solution.py:47
  22.2 2.2 fusion
  24.5 73.9 %all-gather.13.cloned.1.call-done = bf16[2048,1024]{1,0:T(8,128)(2,1)} async-done(((bf16[256,1024]{1,0:T(8,128)(2,1)}), bf16[2048,1024]{1,0:T(8,128)(2,1)}) %all-gather.13.cloned.1.call-update) | async-done | bytes 4194320 | tf_op jit(solution)/shard_map/all_gather | solution.py:55
  98.3 4.6 convolution_convert_fusion.4
  102.9 1.0 fusion.34
  103.9 2.5 all-reduce.2
  106.4 1.0 add_convert_fusion.2
  107.4 2.3 reshape.102
  109.7 2.6 bitcast_add_fusion
  112.4 3.0 copy.24
  115.3 3.5 reshape.103
  118.8 53.0 %all-gather.11.cloned.1.call-done = bf16[2048,1024]{1,0:T(8,128)(2,1)} async-done(((bf16[256,1024]{1,0:T(8,128)(2,1)}), bf16[2048,1024]{1,0:T(8,128)(2,1)}) %all-gather.11.cloned.1.call-update) | async-done | bytes 4194320 | tf_op jit(solution)/shard_map/all_gather | solution.py:54
  171.8 5.2 convolution_convert_fusion.5
  177.0 69.9 %all-gather.15.cloned.1.call-done = bf16[1024,2048]{1,0:T(8,128)(2,1)} async-done(((bf16[1024,256]{1,0:T(8,128)(2,1)}), bf16[1024,2048]{1,0:T(8,128)(2,1)}) %all-gather.15.cloned.1.call-update) | async-done | bytes 4194320 | tf_op jit(solution)/shard_map/all_gather | solution.py:76
  246.9 6.2 %convolution_convert_fusion = bf16[512,2048]{1,0:T(8,128)(2,1)} fusion(bf16[1024,2048]{1,0:T(8,128)(2,1)} %all-gather.15.cloned.1.call-done, f32[512,1024]{1,0:T(8,128)S(1)} %reshape.103, bf16[512,1024]{1,0:T(8,128)(2,1)S(1)} %convolution_convert_fusion.5), kind=kOutput, calls=%fused_computation.18 | convolution fusion | flops 2154299392 | bytes 9437184 | tf_op jit(solution)/shard_map/dot_general | solution.py:79
  253.1 0.2 all-gather.17.cloned.1.call-start
  253.4 7.9 %reduce-scatter.3.cloned.1.call-done = bf16[256,2048]{1,0:T(8,128)(2,1)} async-done(((bf16[512,2048]{1,0:T(8,128)(2,1)}), bf16[256,2048]{1,0:T(8,128)(2,1)}) %reduce-scatter.3.cloned.1.call-update) | async-done | bytes 1048592 | tf_op jit(solution)/shard_map/reduce_scatter | solution.py:78
  261.2 2.6 add_convert_fusion.1
  263.8 0.0 all-gather.19.cloned.1.call-start
  263.9 0.7 all-gather.19.cloned.1.call-update
  264.6 0.0 all-gather.21.cloned.1.call-start
  264.6 0.7 all-gather.21.cloned.1.call-update
  265.3 0.0 all-gather.23.cloned.1.call-start
  265.4 0.7 all-gather.23.cloned.1.call-update
  266.1 0.0 reduce-scatter.5.cloned.1.call-start
  266.1 1.6 dynamic-slice_reduce_fusion.2
  267.7 0.5 fusion.47
  268.2 7.6 %all-gather.17.cloned.1.call-done = bf16[512,2048]{1,0:T(8,128)(2,1)} async-done(((bf16[256,2048]{1,0:T(8,128)(2,1)}), bf16[512,2048]{1,0:T(8,128)(2,1)}) %all-gather.17.cloned.1.call-update) | async-done | bytes 2097168 | tf_op jit(solution)/shard_map/all_gather | solution.py:85
  275.9 2.2 fusion.3
  278.1 93.5 %all-gather.19.cloned.1.call-done = bf16[2048,1408]{1,0:T(8,128)(2,1)} async-done(((bf16[256,1408]{1,0:T(8,128)(2,1)}), bf16[2048,1408]{1,0:T(8,128)(2,1)}) %all-gather.19.cloned.1.call-update) | async-done | bytes 5767184 | tf_op jit(solution)/shard_map/all_gather | solution.py:91
  371.6 6.1 %convolution_convert_fusion.2 = bf16[512,1408]{1,0:T(8,128)(2,1)S(1)} fusion(bf16[2048,1408]{1,0:T(8,128)(2,1)} %all-gather.19.cloned.1.call-done, bf16[512,2048]{1,0:T(8,128)(2,1)S(1)} %copy-done.5, f32[2048]{0:T(1024)} %param.23, f32[512]{0:T(512)S(1)} %add_rsqrt_fusion), kind=kOutput, calls=%fused_computation.20 | convolution fusion | flops 2957705216 | bytes 9316352 | tf_op jit(solution)/shard_map/dot_general | solution.py:25
  377.7 1.7 slice.20
  379.4 1.8 slice.21
  381.2 83.0 %all-gather.21.cloned.1.call-done = bf16[2048,1408]{1,0:T(8,128)(2,1)} async-done(((bf16[256,1408]{1,0:T(8,128)(2,1)}), bf16[2048,1408]{1,0:T(8,128)(2,1)}) %all-gather.21.cloned.1.call-update) | async-done | bytes 5767184 | tf_op jit(solution)/shard_map/all_gather | solution.py:92
  464.3 7.3 %convolution_convert_fusion.1 = bf16[512,1408]{1,0:T(8,128)(2,1)} fusion(bf16[2048,1408]{1,0:T(8,128)(2,1)} %all-gather.21.cloned.1.call-done, bf16[512,2048]{1,0:T(8,128)(2,1)S(1)} %copy-done.5, f32[2048]{0:T(1024)} %param.23, f32[512]{0:T(512)S(1)} %add_rsqrt_fusion), kind=kOutput, calls=%fused_computation.19 | convolution fusion | flops 2957705216 | bytes 9316352 | tf_op jit(solution)/shard_map/dot_general | solution.py:26
  471.6 86.1 %all-gather.23.cloned.1.call-done = bf16[1408,2048]{1,0:T(8,128)(2,1)} async-done(((bf16[1408,256]{1,0:T(8,128)(2,1)}), bf16[1408,2048]{1,0:T(8,128)(2,1)}) %all-gather.23.cloned.1.call-update) | async-done | bytes 5767184 | tf_op jit(solution)/shard_map/all_gather | solution.py:105
  557.7 11.1 %convolution_convert_fusion.3 = bf16[512,2048]{1,0:T(8,128)(2,1)} fusion(bf16[1408,2048]{1,0:T(8,128)(2,1)} %all-gather.23.cloned.1.call-done, bf16[512,1408]{1,0:T(8,128)(2,1)} %convolution_convert_fusion.1, f32[510,1408]{1,0:T(8,128)} %slice.21, f32[511,1408]{1,0:T(8,128)} %slice.20, f32[1408]{0:T(1024)} %get-tuple-element.9, f32[1408]{0:T(1024)} %get-tuple-element.8, ...), kind=kOutput, calls=%fused_computation.21 | convolution fusion | flops 2964652032 | bytes 16516096 | tf_op jit(solution)/shard_map/dot_general | solution.py:108
  568.8 8.1 %reduce-scatter.5.cloned.1.call-done = bf16[256,2048]{1,0:T(8,128)(2,1)} async-done(((bf16[512,2048]{1,0:T(8,128)(2,1)}), bf16[256,2048]{1,0:T(8,128)(2,1)}) %reduce-scatter.5.cloned.1.call-update) | async-done | bytes 1048592 | tf_op jit(solution)/shard_map/reduce_scatter | solution.py:107
  576.9 2.6 add_convert_fusion
  (31 shorter events, 0.1 us)
Async XLA Ops:
  6.5 2.9 copy-start
  6.5 15.7 %all-gather.9.cloned.1.call-start = ((), (), s32[]{:S(2)}) async-start(), calls=%async_computation.2 | async-start | bytes 3145728 | tf_op jit(solution)/shard_map/all_gather | solution.py:47
  7.3 91.1 %copy-start.7 = (f32[2048]{0:T(1024)S(1)}, f32[2048]{0:T(1024)}, u32[]{:S(2)}) copy-start(f32[2048]{0:T(1024)} %param.15) | copy-start | bytes 24580
  7.3 91.1 %all-gather.13.cloned.1.call-start = ((), (), s32[]{:S(2)}) async-start(), calls=%async_computation.4 | async-start | bytes 4718592 | tf_op jit(solution)/shard_map/all_gather | solution.py:55
  8.0 163.8 %all-gather.11.cloned.1.call-start = ((), (), s32[]{:S(2)}) async-start(), calls=%async_computation.3 | async-start | bytes 4718592 | tf_op jit(solution)/shard_map/all_gather | solution.py:54
  8.8 238.2 %all-gather.15.cloned.1.call-start = ((), (), s32[]{:S(2)}) async-start(), calls=%async_computation.5 | async-start | bytes 4718592 | tf_op jit(solution)/shard_map/all_gather | solution.py:76
  9.3 251.9 %reduce-scatter.3.cloned.1.call-start = ((), (), s32[]{:S(2)}) async-start(), calls=%async_computation.6 | async-start | bytes 3145728 | tf_op jit(solution)/shard_map/reduce_scatter | solution.py:78
  22.2 76.1 %copy-start.4 = (bf16[512,2048]{1,0:T(8,128)(2,1)S(1)}, bf16[512,2048]{1,0:T(8,128)(2,1)}, u32[]{:S(2)}) copy-start(bf16[512,2048]{1,0:T(8,128)(2,1)} %all-gather.9.cloned.1.call-done) | copy-start | bytes 6291460
  24.4 81.9 %dynamic-slice-start = ((f32[2048]{0:T(1024)}, s32[]{:T(128)}), f32[1024]{0:T(1024)S(1)}, s32[]{:S(2)}) async-start(f32[2048]{0:T(1024)} %param.18, s32[]{:T(128)} %select_n.51), calls=%async_computation.12 | async-start | bytes 8704 | tf_op jit(solution)/shard_map/dynamic_slice | solution.py:63
  24.5 81.9 %dynamic-slice-start.1 = ((f32[2048]{0:T(1024)}, s32[]{:T(128)}), f32[1024]{0:T(1024)S(1)}, s32[]{:S(2)}) async-start(f32[2048]{0:T(1024)} %param.19, s32[]{:T(128)} %select_n.51), calls=%async_computation.13 | async-start | bytes 8704 | tf_op jit(solution)/shard_map/dynamic_slice | solution.py:64
  107.4 2.3 copy-start.6
  253.1 8.1 %copy-start.3 = (bf16[256,2048]{1,0:T(8,128)(2,1)S(1)}, bf16[256,2048]{1,0:T(8,128)(2,1)}, u32[]{:S(2)}) copy-start(bf16[256,2048]{1,0:T(8,128)(2,1)} %param.14) | copy-start | bytes 3145732
  253.1 22.7 %all-gather.17.cloned.1.call-start = ((), (), s32[]{:S(2)}) async-start(), calls=%async_computation.7 | async-start | bytes 3145728 | tf_op jit(solution)/shard_map/all_gather | solution.py:85
  263.8 107.7 %all-gather.19.cloned.1.call-start = ((), (), s32[]{:S(2)}) async-start(), calls=%async_computation.8 | async-start | bytes 6488064 | tf_op jit(solution)/shard_map/all_gather | solution.py:91
  264.6 199.7 %all-gather.21.cloned.1.call-start = ((), (), s32[]{:S(2)}) async-start(), calls=%async_computation.9 | async-start | bytes 6488064 | tf_op jit(solution)/shard_map/all_gather | solution.py:92
  265.3 292.3 %all-gather.23.cloned.1.call-start = ((), (), s32[]{:S(2)}) async-start(), calls=%async_computation.10 | async-start | bytes 6488064 | tf_op jit(solution)/shard_map/all_gather | solution.py:105
  266.1 310.8 %reduce-scatter.5.cloned.1.call-start = ((), (), s32[]{:S(2)}) async-start(), calls=%async_computation.11 | async-start | bytes 3145728 | tf_op jit(solution)/shard_map/reduce_scatter | solution.py:107
  275.9 95.7 %copy-start.5 = (bf16[512,2048]{1,0:T(8,128)(2,1)S(1)}, bf16[512,2048]{1,0:T(8,128)(2,1)}, u32[]{:S(2)}) copy-start(bf16[512,2048]{1,0:T(8,128)(2,1)} %all-gather.17.cloned.1.call-done) | copy-start | bytes 6291460
  381.2 176.4 %copy-start.8 = (pred[512]{0:T(512)(128)(4,1)S(1)}, pred[512]{0:T(512)(128)(4,1)}, u32[]{:S(2)}) copy-start(pred[512]{0:T(512)(128)(4,1)} %get-tuple-element.14) | copy-start | bytes 1540
  568.8 8.1 %copy-start.2 = (bf16[256,2048]{1,0:T(8,128)(2,1)S(1)}, bf16[256,2048]{1,0:T(8,128)(2,1)}, u32[]{:S(2)}) copy-start(bf16[256,2048]{1,0:T(8,128)(2,1)} %add_convert_fusion.1) | copy-start | bytes 3145732
  568.8 10.7 %copy-start.1 = (f32[32,128]{1,0:T(8,128)S(1)}, f32[32,128]{1,0:T(8,128)}, u32[]{:S(2)}) copy-start(f32[32,128]{1,0:T(8,128)} %param.21) | copy-start | bytes 49156
Sparse Core Ops, SparseCore 0:
  8.9 13.2 all-gather.8
  24.3 73.9 all-gather.12
  100.5 71.3 all-gather.10
  173.7 73.1 all-gather.14
  253.3 7.9 reduce-scatter.2
  264.0 11.8 all-gather.16
  278.0 93.4 all-gather.18
  373.7 90.4 all-gather.20
  466.3 91.3 all-gather.22
  569.0 7.9 reduce-scatter.4
where the time goes:
time: 587 us; the launch traced here: 586 us
  waiting for transfers between devices  500 us (85%)
  matrix products  43.1 us (7%)
  local copies, waits for them, and re-layouts  14 us (2%)
  between operations  13.7 us (2%)
  other arithmetic  12.2 us (2%)
    all_gather x1, waiting for transfers between devices, on_device(): lax.all_gather(gate_proj, 'fs', axis=0, tiled=True)  93.5 us
    all_gather x1, waiting for transfers between devices, on_device(): down_whole = lax.all_gather(down_proj, 'fs', axis=1, tiled=True)  86.1 us
    all_gather x1, waiting for transfers between devices, on_device(): lax.all_gather(up_proj, 'fs', axis=0, tiled=True)  83 us
    all_gather x1, waiting for transfers between devices, on_device(): lax.all_gather(spatial_proj, 'fs', axis=0, tiled=True)  73.9 us
    all_gather x1, waiting for transfers between devices, on_device(): out_whole = lax.all_gather(mixer_out, 'fs', axis=1, tiled=True)  69.9 us
    all_gather x1, waiting for transfers between devices, on_device(): lax.all_gather(gating_proj, 'fs', axis=0, tiled=True)  53 us
    all_gather x1, waiting for transfers between devices, on_device(): rows = lax.all_gather(residual, 'tp', axis=0, tiled=True)  12.7 us
    dot_general x2, matrix products, fold_pair(): second = jnp.dot(normed, pieces[1], preferred_element_type=jnp.float32)  11.9 us
  transfers between devices with their start and end apart: 10, of which 10 were waited for; matrix products, arithmetic and copies ran while one was open for 8% of the time, Pallas kernels for 0%

commit v1 on v0

--- a/solution.py
+++ b/solution.py
@@ -102,7 +102,12 @@
         shifted = jnp.where((offset >= lag)[:, None], shifted, 0.0)
         conv = conv + taps_here[KCONV - 1 - lag] * shifted
     hidden = (jax.nn.silu(conv) * up).astype(jnp.bfloat16)
-    down_whole = lax.all_gather(down_proj, "fs", axis=1, tiled=True)
+    ring = [down_proj]
+    for hop in range(7):
+        ring.append(lax.ppermute(ring[-1], "fs", [(dev, (dev + 1) % 8) for dev in range(8)]))
+    down_whole = jnp.roll(
+        jnp.concatenate(ring[::-1], axis=1), (lax.axis_index("fs") + 1) * ring[0].shape[1], axis=1
+    )
     part = hidden
     channel_part = lax.psum_scatter(
         jnp.dot(part, down_whole, preferred_element_type=jnp.float32).astype(jnp.bfloat16),

time: 587 us -> 567 us (0.966)
  waiting for transfers between devices: 500 us -> 457 us
  local copies, waits for them, and re-layouts: 14 us -> 35.3 us
    ppermute x0 -> x7, waiting for transfers between devices: none -> 204 us  [on_device(): lax.ppermute(ring[-1], 'fs', [(dev, (dev + 1) % 8) for dev in range(8)])]
    all_gather x1, waiting for transfers between devices: 93.5 us -> 0.02 us  [on_device(): lax.all_gather(gate_proj, 'fs', axis=0, tiled=True)]
    all_gather x1 -> x0, waiting for transfers between devices: 86.1 us -> none  [on_device(): down_whole = lax.all_gather(down_proj, 'fs', axis=1, tiled=True)]
    all_gather x1, waiting for transfers between devices: 83 us -> 26.1 us  [on_device(): lax.all_gather(up_proj, 'fs', axis=0, tiled=True)]
    unnamed x18 -> x43, local copies, waits for them, and re-layouts: 0.04 us -> 20.9 us
    all_gather x1, waiting for transfers between devices: 7.65 us -> 0.01 us  [on_device(): rows2 = lax.all_gather(middle, 'tp', axis=0, tiled=True)]
  transfers between devices with their start and end apart: 10 -> 16, of which waited for: 10 -> 14; matrix products, arithmetic and copies ran while one was open for 8% -> 11% of each run, Pallas kernels for 0% -> 0%
where the time goes in v1:
time: 567 us; the launch traced here: 566 us
  waiting for transfers between devices  457 us (81%)
  matrix products  43.6 us (8%)
  local copies, waits for them, and re-layouts  35.3 us (6%)
  between operations  13.4 us (2%)
  other arithmetic  11.4 us (2%)
    ppermute x7, waiting for transfers between devices, on_device(): lax.ppermute(ring[-1], 'fs', [(dev, (dev + 1) % 8) for dev in range(8)])  204 us
    all_gather x1, waiting for transfers between devices, on_device(): lax.all_gather(spatial_proj, 'fs', axis=0, tiled=True)  74 us
    all_gather x1, waiting for transfers between devices, on_device(): out_whole = lax.all_gather(mixer_out, 'fs', axis=1, tiled=True)  68.9 us
    all_gather x1, waiting for transfers between devices, on_device(): lax.all_gather(gating_proj, 'fs', axis=0, tiled=True)  52.2 us
    all_gather x1, waiting for transfers between devices, on_device(): lax.all_gather(up_proj, 'fs', axis=0, tiled=True)  26.1 us
    unnamed x43, local copies, waits for them, and re-layouts  20.9 us
    dot_general x2, matrix products, fold_pair(): first = jnp.dot(normed, pieces[0], preferred_element_type=jnp.float32)  12.9 us
    all_gather x1, waiting for transfers between devices, on_device(): rows = lax.all_gather(residual, 'tp', axis=0, tiled=True)  12.7 us
  transfers between devices with their start and end apart: 16, of which 14 were waited for; matrix products, arithmetic and copies ran while one was open for 11% of the time, Pallas kernels for 0%

profile of v1, /device:TPU:0, one launch (start us, length us, event | category | flops | bytes accessed | tf_op | source)
XLA Modules:
  0.0 566.0 jit_solution(15447162905289532325)
XLA Ops:
  9.5 12.7 %all-gather.8.cloned.1.call-done = bf16[512,2048]{1,0:T(8,128)(2,1)} async-done(((bf16[256,2048]{1,0:T(8,128)(2,1)}), bf16[512,2048]{1,0:T(8,128)(2,1)}) %all-gather.8.cloned.1.call-update) | async-done | bytes 2097168 | tf_op jit(solution)/shard_map/all_gather | solution.py:47
  22.2 2.1 fusion.2
  24.3 74.0 %all-gather.12.cloned.1.call-done = bf16[2048,1024]{1,0:T(8,128)(2,1)} async-done(((bf16[256,1024]{1,0:T(8,128)(2,1)}), bf16[2048,1024]{1,0:T(8,128)(2,1)}) %all-gather.12.cloned.1.call-update) | async-done | bytes 4194320 | tf_op jit(solution)/shard_map/all_gather | solution.py:55
  98.3 5.2 convolution_convert_fusion.3
  103.5 1.0 fusion.39
  104.5 2.6 all-reduce.2
  107.1 1.0 add_convert_fusion.2
  108.2 2.3 reshape.102
  110.5 2.6 bitcast_add_fusion
  113.1 3.0 copy.24
  116.1 3.5 reshape.103
  119.6 52.2 %all-gather.10.cloned.1.call-done = bf16[2048,1024]{1,0:T(8,128)(2,1)} async-done(((bf16[256,1024]{1,0:T(8,128)(2,1)}), bf16[2048,1024]{1,0:T(8,128)(2,1)}) %all-gather.10.cloned.1.call-update) | async-done | bytes 4194320 | tf_op jit(solution)/shard_map/all_gather | solution.py:54
  171.8 6.2 %convolution_convert_fusion.4 = bf16[512,1024]{1,0:T(8,128)(2,1)} fusion(bf16[2048,1024]{1,0:T(8,128)(2,1)} %all-gather.10.cloned.1.call-done, bf16[512,2048]{1,0:T(8,128)(2,1)} %all-gather.8.cloned.1.call-done, f32[2048]{0:T(1024)S(1)} %copy-done.12, f32[512]{0:T(512)S(1)} %add_rsqrt_fusion.2), kind=kOutput, calls=%fused_computation.45 | convolution fusion | flops 2152202240 | bytes 7350272 | tf_op jit(solution)/shard_map/dot_general | solution.py:25
  178.0 68.9 %all-gather.14.cloned.1.call-done = bf16[1024,2048]{1,0:T(8,128)(2,1)} async-done(((bf16[1024,256]{1,0:T(8,128)(2,1)}), bf16[1024,2048]{1,0:T(8,128)(2,1)}) %all-gather.14.cloned.1.call-update) | async-done | bytes 4194320 | tf_op jit(solution)/shard_map/all_gather | solution.py:76
  246.9 6.5 %convolution_convert_fusion = bf16[512,2048]{1,0:T(8,128)(2,1)} fusion(bf16[1024,2048]{1,0:T(8,128)(2,1)} %all-gather.14.cloned.1.call-done, f32[512,1024]{1,0:T(8,128)S(1)} %reshape.103, bf16[512,1024]{1,0:T(8,128)(2,1)} %convolution_convert_fusion.4), kind=kOutput, calls=%fused_computation.20 | convolution fusion | flops 2154299392 | bytes 9437184 | tf_op jit(solution)/shard_map/dot_general | solution.py:79
  253.7 7.9 %reduce-scatter.3.cloned.1.call-done = bf16[256,2048]{1,0:T(8,128)(2,1)} async-done(((bf16[512,2048]{1,0:T(8,128)(2,1)}), bf16[256,2048]{1,0:T(8,128)(2,1)}) %reduce-scatter.3.cloned.1.call-update) | async-done | bytes 1048592 | tf_op jit(solution)/shard_map/reduce_scatter | solution.py:78
  261.5 2.6 add_convert_fusion.1
  265.0 1.9 collective-permute-start
  266.9 19.1 %collective-permute-done = bf16[1408,256]{1,0:T(8,128)(2,1)S(1)} collective-permute-done((bf16[1408,256]{1,0:T(8,128)(2,1)S(1)}, bf16[1408,256]{1,0:T(8,128)(2,1)S(1)}, u32[]{:S(2)}, u32[]{:S(2)}) %collective-permute-start) | collective-permute-done | bytes 720928 | tf_op jit(solution)/shard_map/ppermute | solution.py:107
  286.1 34.5 %collective-permute-done.1 = bf16[1408,256]{1,0:T(8,128)(2,1)S(1)} collective-permute-done((bf16[1408,256]{1,0:T(8,128)(2,1)S(1)}, bf16[1408,256]{1,0:T(8,128)(2,1)S(1)}, u32[]{:S(2)}, u32[]{:S(2)}) %collective-permute-start.1) | collective-permute-done | bytes 720928 | tf_op jit(solution)/shard_map/ppermute | solution.py:107
  320.6 26.9 %collective-permute-done.2 = bf16[1408,256]{1,0:T(8,128)(2,1)S(1)} collective-permute-done((bf16[1408,256]{1,0:T(8,128)(2,1)S(1)}, bf16[1408,256]{1,0:T(8,128)(2,1)S(1)}, u32[]{:S(2)}, u32[]{:S(2)}) %collective-permute-start.2) | collective-permute-done | bytes 720928 | tf_op jit(solution)/shard_map/ppermute | solution.py:107
  347.5 35.5 %collective-permute-done.3 = bf16[1408,256]{1,0:T(8,128)(2,1)S(1)} collective-permute-done((bf16[1408,256]{1,0:T(8,128)(2,1)S(1)}, bf16[1408,256]{1,0:T(8,128)(2,1)S(1)}, u32[]{:S(2)}, u32[]{:S(2)}) %collective-permute-start.3) | collective-permute-done | bytes 720928 | tf_op jit(solution)/shard_map/ppermute | solution.py:107
  383.9 35.3 %collective-permute-done.4 = bf16[1408,256]{1,0:T(8,128)(2,1)S(1)} collective-permute-done((bf16[1408,256]{1,0:T(8,128)(2,1)S(1)}, bf16[1408,256]{1,0:T(8,128)(2,1)S(1)}, u32[]{:S(2)}, u32[]{:S(2)}) %collective-permute-start.4) | collective-permute-done | bytes 720928 | tf_op jit(solution)/shard_map/ppermute | solution.py:107
  420.0 17.9 %collective-permute-done.5 = bf16[1408,256]{1,0:T(8,128)(2,1)} collective-permute-done((bf16[1408,256]{1,0:T(8,128)(2,1)S(1)}, bf16[1408,256]{1,0:T(8,128)(2,1)}, u32[]{:S(2)}, u32[]{:S(2)}) %collective-permute-start.5) | collective-permute-done | bytes 720928 | tf_op jit(solution)/shard_map/ppermute | solution.py:107
  438.0 1.0 dynamic-slice_reduce_fusion.2
  438.9 34.8 %collective-permute-done.6 = bf16[1408,256]{1,0:T(8,128)(2,1)} collective-permute-done((bf16[1408,256]{1,0:T(8,128)(2,1)}, bf16[1408,256]{1,0:T(8,128)(2,1)}, u32[]{:S(2)}, u32[]{:S(2)}) %collective-permute-start.6) | collective-permute-done | bytes 720928 | tf_op jit(solution)/shard_map/ppermute | solution.py:107
  473.7 2.1 constant_dynamic-update-slice_fusion.15
  475.8 2.1 constant_dynamic-update-slice_fusion.14
  477.9 1.0 constant_dynamic-update-slice_fusion.13
  478.9 1.0 constant_dynamic-update-slice_fusion.12
  479.9 1.0 constant_dynamic-update-slice_fusion.11
  480.9 1.0 constant_dynamic-update-slice_fusion.10
  481.9 1.0 constant_dynamic-update-slice_fusion.9
  482.8 1.0 constant_dynamic-update-slice_fusion.8
  483.8 2.1 constant_dynamic-update-slice_fusion.7
  485.9 2.1 constant_dynamic-update-slice_fusion.6
  489.9 1.0 constant_dynamic-update-slice_fusion.3
  490.9 1.0 constant_dynamic-update-slice_fusion.2
  491.8 1.0 constant_dynamic-update-slice_fusion.1
  493.8 2.1 fusion.5
  495.9 6.7 %convolution_convert_fusion.2 = bf16[512,1408]{1,0:T(8,128)(2,1)S(1)} fusion(bf16[2048,1408]{1,0:T(8,128)(2,1)} %all-gather.18.cloned.1.call-done, bf16[512,2048]{1,0:T(8,128)(2,1)} %all-gather.16.cloned.1.call-done, f32[2048]{0:T(1024)S(1)} %copy-done.13, f32[512]{0:T(512)S(1)} %add_rsqrt_fusion), kind=kOutput, calls=%fused_computation.23 | convolution fusion | flops 2957705216 | bytes 9316352 | tf_op jit(solution)/shard_map/dot_general | solution.py:25
  502.7 1.8 slice.21
  504.4 1.8 slice.20
  506.2 26.1 %all-gather.20.cloned.1.call-done = bf16[2048,1408]{1,0:T(8,128)(2,1)} async-done(((bf16[256,1408]{1,0:T(8,128)(2,1)}), bf16[2048,1408]{1,0:T(8,128)(2,1)}) %all-gather.20.cloned.1.call-update) | async-done | bytes 5767184 | tf_op jit(solution)/shard_map/all_gather | solution.py:92
  532.3 6.9 %convolution_convert_fusion.1 = bf16[512,1408]{1,0:T(8,128)(2,1)S(1)} fusion(bf16[2048,1408]{1,0:T(8,128)(2,1)} %all-gather.20.cloned.1.call-done, bf16[512,2048]{1,0:T(8,128)(2,1)} %all-gather.16.cloned.1.call-done, f32[2048]{0:T(1024)S(1)} %copy-done.13, f32[512]{0:T(512)S(1)} %add_rsqrt_fusion), kind=kOutput, calls=%fused_computation.22 | convolution fusion | flops 2957705216 | bytes 9316352 | tf_op jit(solution)/shard_map/dot_general | solution.py:26
  539.2 9.5 %fusion.8 = bf16[512,2048]{1,0:T(8,128)(2,1)} fusion(bf16[1408,4096]{1,0:T(8,128)(2,1)} %constant_dynamic-update-slice_fusion, s32[]{:T(128)S(6)} %select_n.72, bf16[512,1408]{1,0:T(8,128)(2,1)S(1)} %convolution_convert_fusion.1, f32[510,1408]{1,0:T(8,128)S(1)} %copy-done.4, f32[511,1408]{1,0:T(8,128)S(1)} %copy-done.5, f32[1408]{0:T(1024)S(1)} %get-tuple-element.9, ...), kind=kOutput, calls=%fused_computation.21 | convolution fusion | flops 2964652032 | bytes 16516100 | tf_op jit(solution)/shard_map/dot_general | solution.py:113
  548.8 8.1 %reduce-scatter.5.cloned.1.call-done = bf16[256,2048]{1,0:T(8,128)(2,1)} async-done(((bf16[512,2048]{1,0:T(8,128)(2,1)}), bf16[256,2048]{1,0:T(8,128)(2,1)}) %reduce-scatter.5.cloned.1.call-update) | async-done | bytes 1048592 | tf_op jit(solution)/shard_map/reduce_scatter | solution.py:112
  556.9 2.6 add_convert_fusion
  (68 shorter events, 8.7 us)
Async XLA Ops:
  6.5 2.9 copy-start
  6.5 91.8 %copy-start.12 = (f32[2048]{0:T(1024)S(1)}, f32[2048]{0:T(1024)}, u32[]{:S(2)}) copy-start(f32[2048]{0:T(1024)} %param.15) | copy-start | bytes 24580
  6.5 15.7 %all-gather.8.cloned.1.call-start = ((), (), s32[]{:S(2)}) async-start(), calls=%async_computation.2 | async-start | bytes 3145728 | tf_op jit(solution)/shard_map/all_gather | solution.py:47
  7.3 91.1 %all-gather.12.cloned.1.call-start = ((), (), s32[]{:S(2)}) async-start(), calls=%async_computation.4 | async-start | bytes 4718592 | tf_op jit(solution)/shard_map/all_gather | solution.py:55
  8.0 163.8 %all-gather.10.cloned.1.call-start = ((), (), s32[]{:S(2)}) async-start(), calls=%async_computation.3 | async-start | bytes 4718592 | tf_op jit(solution)/shard_map/all_gather | solution.py:54
  8.7 238.2 %all-gather.14.cloned.1.call-start = ((), (), s32[]{:S(2)}) async-start(), calls=%async_computation.5 | async-start | bytes 4718592 | tf_op jit(solution)/shard_map/all_gather | solution.py:76
  9.3 252.2 %reduce-scatter.3.cloned.1.call-start = ((), (), s32[]{:S(2)}) async-start(), calls=%async_computation.6 | async-start | bytes 3145728 | tf_op jit(solution)/shard_map/reduce_scatter | solution.py:78
  24.3 82.8 %dynamic-slice-start = ((f32[2048]{0:T(1024)}, s32[]{:T(128)}), f32[1024]{0:T(1024)S(1)}, s32[]{:S(2)}) async-start(f32[2048]{0:T(1024)} %param.19, s32[]{:T(128)} %select_n.63), calls=%async_computation.11 | async-start | bytes 8704 | tf_op jit(solution)/shard_map/dynamic_slice | solution.py:64
  24.3 82.8 %dynamic-slice-start.1 = ((f32[2048]{0:T(1024)}, s32[]{:T(128)}), f32[1024]{0:T(1024)S(1)}, s32[]{:S(2)}) async-start(f32[2048]{0:T(1024)} %param.18, s32[]{:T(128)} %select_n.63), calls=%async_computation.12 | async-start | bytes 8704 | tf_op jit(solution)/shard_map/dynamic_slice | solution.py:63
  104.5 6.0 %copy-start.11 = (bf16[32,128,128]{2,1,0:T(8,128)(2,1)S(1)}, bf16[32,128,128]{2,1,0:T(8,128)(2,1)}, u32[]{:S(2)}) copy-start(bf16[32,128,128]{2,1,0:T(8,128)(2,1)} %param.20) | copy-start | bytes 3145732
  178.0 83.6 %copy-start.3 = (bf16[256,2048]{1,0:T(8,128)(2,1)S(1)}, bf16[256,2048]{1,0:T(8,128)(2,1)}, u32[]{:S(2)}) copy-start(bf16[256,2048]{1,0:T(8,128)(2,1)} %param.14) | copy-start | bytes 3145732
  253.4 11.5 %copy-start.6 = (bf16[1408,256]{1,0:T(8,128)(2,1)S(1)}, bf16[1408,256]{1,0:T(8,128)(2,1)}, u32[]{:S(2)}) copy-start(bf16[1408,256]{1,0:T(8,128)(2,1)} %param.27) | copy-start | bytes 2162692
  253.5 240.3 %all-gather.16.cloned.1.call-start = ((), (), s32[]{:S(2)}) async-start(), calls=%async_computation.7 | async-start | bytes 3145728 | tf_op jit(solution)/shard_map/all_gather | solution.py:85
  264.2 231.7 %all-gather.18.cloned.1.call-start = ((), (), s32[]{:S(2)}) async-start(), calls=%async_computation.8 | async-start | bytes 6488064 | tf_op jit(solution)/shard_map/all_gather | solution.py:91
  264.9 267.4 %all-gather.20.cloned.1.call-start = ((), (), s32[]{:S(2)}) async-start(), calls=%async_computation.9 | async-start | bytes 6488064 | tf_op jit(solution)/shard_map/all_gather | solution.py:92
  265.0 21.1 %collective-permute-start = (bf16[1408,256]{1,0:T(8,128)(2,1)S(1)}, bf16[1408,256]{1,0:T(8,128)(2,1)S(1)}, u32[]{:S(2)}, u32[]{:S(2)}) collective-permute-start(bf16[1408,256]{1,0:T(8,128)(2,1)S(1)} %copy-done.6), channel_id=1, source_target_pairs={{0,2},{2,4},{4,6},{6,8},{8,10},{10,12},{12,14},{14,0},{1,3},{3,5},... | collective-permute-start | bytes 2162696 | tf_op jit(solution)/shard_map/ppermute | solution.py:107
  266.9 290.0 %reduce-scatter.5.cloned.1.call-start = ((), (), s32[]{:S(2)}) async-start(), calls=%async_computation.10 | async-start | bytes 3145728 | tf_op jit(solution)/shard_map/reduce_scatter | solution.py:112
  286.1 34.5 %collective-permute-start.1 = (bf16[1408,256]{1,0:T(8,128)(2,1)S(1)}, bf16[1408,256]{1,0:T(8,128)(2,1)S(1)}, u32[]{:S(2)}, u32[]{:S(2)}) collective-permute-start(bf16[1408,256]{1,0:T(8,128)(2,1)S(1)} %collective-permute-done), channel_id=1, source_target_pairs={{0,2},{2,4},{4,6},{6,8},{8,10},{10,12},{12,14},{14,0},{1,3},{3,5},... | collective-permute-start | bytes 2162696 | tf_op jit(solution)/shard_map/ppermute | solution.py:107
  320.6 26.9 %collective-permute-start.2 = (bf16[1408,256]{1,0:T(8,128)(2,1)S(1)}, bf16[1408,256]{1,0:T(8,128)(2,1)S(1)}, u32[]{:S(2)}, u32[]{:S(2)}) collective-permute-start(bf16[1408,256]{1,0:T(8,128)(2,1)S(1)} %collective-permute-done.1), channel_id=1, source_target_pairs={{0,2},{2,4},{4,6},{6,8},{8,10},{10,12},{12,14},{14,0},{1,3},{3,5},... | collective-permute-start | bytes 2162696 | tf_op jit(solution)/shard_map/ppermute | solution.py:107
  347.5 35.5 %collective-permute-start.3 = (bf16[1408,256]{1,0:T(8,128)(2,1)S(1)}, bf16[1408,256]{1,0:T(8,128)(2,1)S(1)}, u32[]{:S(2)}, u32[]{:S(2)}) collective-permute-start(bf16[1408,256]{1,0:T(8,128)(2,1)S(1)} %collective-permute-done.2), channel_id=1, source_target_pairs={{0,2},{2,4},{4,6},{6,8},{8,10},{10,12},{12,14},{14,0},{1,3},{3,5},... | collective-permute-start | bytes 2162696 | tf_op jit(solution)/shard_map/ppermute | solution.py:107
  383.0 0.9 copy-start.7
  383.9 35.3 %collective-permute-start.4 = (bf16[1408,256]{1,0:T(8,128)(2,1)S(1)}, bf16[1408,256]{1,0:T(8,128)(2,1)S(1)}, u32[]{:S(2)}, u32[]{:S(2)}) collective-permute-start(bf16[1408,256]{1,0:T(8,128)(2,1)S(1)} %collective-permute-done.3), channel_id=1, source_target_pairs={{0,2},{2,4},{4,6},{6,8},{8,10},{10,12},{12,14},{14,0},{1,3},{3,5},... | collective-permute-start | bytes 2162696 | tf_op jit(solution)/shard_map/ppermute | solution.py:107
  419.2 0.9 copy-start.9
  420.0 17.9 %collective-permute-start.5 = (bf16[1408,256]{1,0:T(8,128)(2,1)S(1)}, bf16[1408,256]{1,0:T(8,128)(2,1)}, u32[]{:S(2)}, u32[]{:S(2)}) collective-permute-start(bf16[1408,256]{1,0:T(8,128)(2,1)S(1)} %collective-permute-done.4), channel_id=1, source_target_pairs={{0,2},{2,4},{4,6},{6,8},{8,10},{10,12},{12,14},{14,0},{1,3},{3,5},... | collective-permute-start | bytes 2162696 | tf_op jit(solution)/shard_map/ppermute | solution.py:107
  437.9 35.8 %collective-permute-start.6 = (bf16[1408,256]{1,0:T(8,128)(2,1)}, bf16[1408,256]{1,0:T(8,128)(2,1)}, u32[]{:S(2)}, u32[]{:S(2)}) collective-permute-start(bf16[1408,256]{1,0:T(8,128)(2,1)} %collective-permute-done.5), channel_id=1, source_target_pairs={{0,2},{2,4},{4,6},{6,8},{8,10},{10,12},{12,14},{14,0},{1,3},{3,5},... | collective-permute-start | bytes 2162696 | tf_op jit(solution)/shard_map/ppermute | solution.py:107
  437.9 40.0 %copy-start.10 = (bf16[1408,256]{1,0:T(8,128)(2,1)S(1)}, bf16[1408,256]{1,0:T(8,128)(2,1)}, u32[]{:S(2)}) copy-start(bf16[1408,256]{1,0:T(8,128)(2,1)} %copy-done.9) | copy-start | bytes 2162692
  437.9 41.0 %copy-start.8 = (bf16[1408,256]{1,0:T(8,128)(2,1)S(1)}, bf16[1408,256]{1,0:T(8,128)(2,1)}, u32[]{:S(2)}) copy-start(bf16[1408,256]{1,0:T(8,128)(2,1)} %copy-done.7) | copy-start | bytes 2162692
  490.9 5.1 copy-start.13
  532.3 6.9 %copy-start.4 = (f32[510,1408]{1,0:T(8,128)S(1)}, f32[510,1408]{1,0:T(8,128)}, u32[]{:S(2)}) copy-start(f32[510,1408]{1,0:T(8,128)} %slice.21) | copy-start | bytes 8616964
  532.3 6.9 %copy-start.5 = (f32[511,1408]{1,0:T(8,128)S(1)}, f32[511,1408]{1,0:T(8,128)}, u32[]{:S(2)}) copy-start(f32[511,1408]{1,0:T(8,128)} %slice.20) | copy-start | bytes 8633860
  539.2 17.7 %copy-start.2 = (bf16[256,2048]{1,0:T(8,128)(2,1)S(1)}, bf16[256,2048]{1,0:T(8,128)(2,1)}, u32[]{:S(2)}) copy-start(bf16[256,2048]{1,0:T(8,128)(2,1)} %add_convert_fusion.1) | copy-start | bytes 3145732
  539.2 20.2 %copy-start.1 = (f32[32,128]{1,0:T(8,128)S(1)}, f32[32,128]{1,0:T(8,128)}, u32[]{:S(2)}) copy-start(f32[32,128]{1,0:T(8,128)} %param.21) | copy-start | bytes 49156
Sparse Core Ops, SparseCore 0:
  8.9 13.2 all-gather.7
  24.3 73.9 all-gather.11
  100.5 71.3 all-gather.9
  173.7 73.1 all-gather.13
  253.6 7.9 reduce-scatter.2
  264.3 11.8 all-gather.15
  278.3 134.3 all-gather.17
  414.9 117.3 all-gather.19
  548.9 7.9 reduce-scatter.4
